TPU v7x, 32 devices: a whole 2x2x4 slice. The times are simulated.
32 devices in a mesh: sp: 8 (over z, y), tp: 4 (over x, core).
Axes of the slice: x: 2, y: 2, z: 4, core: 2. Of those that a mesh axis runs over, the one named last changes fastest.
Arguments:
- query_rows: bfloat16 [4096, 2048], P('sp', 'tp'), may hold values from -40 to 40
- key_rows: bfloat16 [4096, 256], P('sp', 'tp'), may hold values from -6 to 6
- value_rows: bfloat16 [4096, 256], P('sp', 'tp'), may hold values from -12 to 12
- doc_ids: int32 [4096], P('sp'), may hold values from 0 to 3, never falling along the last dimension, each value on 1 to 2048 neighbouring positions
- sink_logit: float32 [32], P('tp'), may hold values from 1 to 6
- residual: bfloat16 [4096, 2048], P('sp'), may hold values from -10 to 10
- out_proj: bfloat16 [2048, 2048], P('tp'), may hold values from -0.25 to 0.25
- mix_gain: float32 [2048], replicated, may hold values from 0.1 to 1.9
- gate_proj: bfloat16 [2048, 5632], P('sp', 'tp'), may hold values from -0.125 to 0.125
- value_proj: bfloat16 [2048, 5632], P('sp', 'tp'), may hold values from -0.125 to 0.125
- gate_taps: float32 [3, 5632], P(None, 'tp'), may hold values from -3 to 3
- value_taps: float32 [3, 5632], P(None, 'tp'), may hold values from -3 to 3
- down_proj: bfloat16 [5632, 2048], P('tp', 'sp'), may hold values from -0.078125 to 0.078125
- final_gain: float32 [2048], P('tp'), may hold values from 0.1 to 1.9
Outputs:
- mixed: bfloat16 [4096, 2048], P('sp', 'tp')
All inputs are finite; a program needn't handle non-finite values.
Results may differ from a plain program's by a relative error of at most 0.012.
Values may be sent and summed in bfloat16 or wider, within the bound.
A program may use at most 128 MiB of HBM per device.

v0:
```python
import math
import jax
import jax.numpy as jnp
from jax import lax
from jax.sharding import PartitionSpec as P

HD = 64
WIN = 128
TAPS = 3
mix_scale = math.sqrt(2.0)
norm_eps = 1e-05


def passed_along(block, axis, distance):
    devices = range(lax.axis_size(axis))
    route = [(i - distance, i) for i in devices if i - distance in devices]
    return lax.ppermute(block, axis, route)


def attend(query_block, key_block, value_block, query_pos, key_pos, query_doc, key_doc, sink):
    head_size = query_block.shape[-1]
    scores = jnp.einsum(
        "qkgd,skd->kgqs", query_block, key_block, preferred_element_type=jnp.float32
    ) * head_size ** (-0.5)
    diff = query_pos[:, None] - key_pos[None, :]
    valid = (
        (diff >= 0)
        & (diff < WIN)
        & (query_doc[:, None] == key_doc[None, :])
        & (key_pos[None, :] >= 0)
    )
    scores = jnp.where(valid[None, None], scores, -1e30)
    top = jnp.maximum(jnp.max(scores, axis=-1, keepdims=True), sink)
    weights = jnp.exp(scores - top)
    total = jnp.sum(weights, axis=-1, keepdims=True) + jnp.exp(sink - top)
    probs = (weights / total).astype(jnp.bfloat16)
    out = jnp.einsum("kgqs,skd->qkgd", probs, value_block, preferred_element_type=jnp.float32)
    return out.astype(jnp.bfloat16)


def depthwise(tail, current, taps, tail_docs, docs):
    extended = jnp.concatenate([tail, current])
    ext_docs = jnp.concatenate([tail_docs, docs])
    lag_rows = tail.shape[0]
    count = current.shape[0]
    total = jnp.zeros(current.shape, jnp.float32)
    for lag in range(lag_rows + 1):
        start = lag_rows - lag
        same = (ext_docs[start : start + count] == docs)[:, None]
        rows = extended[start : start + count].astype(jnp.float32)
        total = total + taps[lag][None, :] * jnp.where(same, rows, 0.0)
    return total


def on_device(
    query_rows,
    key_rows,
    value_rows,
    doc_ids,
    sink_logit,
    residual,
    out_proj,
    mix_gain,
    gate_proj,
    value_proj,
    gate_taps,
    value_taps,
    down_proj,
    final_gain,
):
    rows = query_rows.shape[0]
    kv_local = key_rows.shape[1] // HD
    heads_local = query_rows.shape[1] // HD
    groups = heads_local // kv_local
    offset = lax.axis_index("sp") * rows
    prev_keys, prev_values, prev_docs = passed_along(
        (key_rows[rows - WIN :], value_rows[rows - WIN :], doc_ids[rows - WIN :]), "sp", 1
    )
    all_keys = jnp.concatenate([prev_keys, key_rows]).reshape(rows + WIN, kv_local, HD)
    all_values = jnp.concatenate([prev_values, value_rows]).reshape(rows + WIN, kv_local, HD)
    all_docs = jnp.concatenate([prev_docs, doc_ids])
    key_pos = offset - WIN + jnp.arange(rows + WIN, dtype=jnp.int32)
    query_pos = offset + jnp.arange(rows, dtype=jnp.int32)
    queries = query_rows.reshape(rows, kv_local, groups, HD)
    sink = sink_logit.reshape(kv_local, groups, 1, 1)
    pieces = attend(queries, all_keys, all_values, query_pos, key_pos, doc_ids, all_docs, sink)
    heads = pieces.reshape(rows, heads_local * HD)
    partial_value = jnp.dot(heads, out_proj, preferred_element_type=jnp.float32)
    width = residual.shape[1]
    share = width // lax.axis_size("tp")
    col_start = lax.axis_index("tp") * share
    attn_total = lax.psum(partial_value.astype(jnp.bfloat16), "tp").astype(jnp.float32)
    first_sum = mix_scale * residual.astype(jnp.float32) + attn_total
    mean = jnp.mean(first_sum, axis=1, keepdims=True)
    var = jnp.mean(jnp.square(first_sum - mean), axis=1, keepdims=True)
    normed = ((first_sum - mean) * lax.rsqrt(var + norm_eps) * mix_gain[None, :]).astype(
        jnp.bfloat16
    )
    normed_own = lax.dynamic_slice_in_dim(normed, col_start, share, 1)
    up_gate = jnp.dot(
        normed,
        lax.all_gather(gate_proj, "sp", axis=0, tiled=True),
        preferred_element_type=jnp.float32,
    )
    up_value = jnp.dot(
        normed,
        lax.all_gather(value_proj, "sp", axis=0, tiled=True),
        preferred_element_type=jnp.float32,
    )
    up_gate = up_gate.astype(jnp.bfloat16)
    up_value = up_value.astype(jnp.bfloat16)
    lag_rows = TAPS - 1
    prev_gate, prev_value = passed_along(
        (up_gate[rows - lag_rows :], up_value[rows - lag_rows :]), "sp", 1
    )
    tail_docs = prev_docs[WIN - lag_rows :]
    conv_gate = depthwise(prev_gate, up_gate, gate_taps, tail_docs, doc_ids)
    conv_value = depthwise(prev_value, up_value, value_taps, tail_docs, doc_ids)
    hidden = (jax.nn.gelu(conv_gate) * conv_value).astype(jnp.bfloat16)
    terms = jnp.dot(
        hidden,
        lax.all_gather(down_proj, "sp", axis=1, tiled=True),
        preferred_element_type=jnp.float32,
    )
    ffn_own = lax.psum_scatter(
        terms.astype(jnp.bfloat16), "tp", scatter_dimension=1, tiled=True
    ).astype(jnp.float32)
    second_sum = mix_scale * normed_own.astype(jnp.float32) + ffn_own
    row_sum, row_squares = lax.psum(
        (jnp.sum(second_sum, axis=1), jnp.sum(second_sum * second_sum, axis=1)), "tp"
    )
    mean = row_sum / width
    var = row_squares / width - mean * mean
    return (
        (second_sum - mean[:, None]) * lax.rsqrt(var + norm_eps)[:, None] * final_gain[None, :]
    ).astype(jnp.bfloat16)


def solution(mesh):
    placed = (
        P("sp", "tp"),
        P("sp", "tp"),
        P("sp", "tp"),
        P("sp"),
        P("tp"),
        P("sp", None),
        P("tp", None),
        P(),
        P("sp", "tp"),
        P("sp", "tp"),
        P(None, "tp"),
        P(None, "tp"),
        P("tp", "sp"),
        P("tp"),
    )
    return jax.shard_map(
        on_device, mesh=mesh, in_specs=placed, out_specs=P("sp", "tp"), check_vma=False
    )
```

profile of v0, /device:TPU:0, one launch (start us, length us, event | category | flops | bytes accessed | tf_op | source)
XLA Modules:
  0.0 373.8 jit_solution(1086754709857433635)
XLA Ops:
  7.4 0.8 slice.57
  8.2 4.9 %collective-permute-start.1 = (s32[128]{0:T(128)S(1)}, s32[128]{0:T(128)S(1)}, u32[]{:S(2)}, u32[]{:S(2)}) collective-permute-start(s32[128]{0:T(128)S(1)} %slice.57), channel_id=1, source_target_pairs={{0,4},{4,8},{8,12},{12,16},{16,20},{20,24},{24,28},{1,5},{5,9},{9,... | collective-permute-start | bytes 1544 | tf_op jit(solution)/shard_map/ppermute | solution.py:17
  13.1 0.7 slice.58
  13.8 3.4 collective-permute-start.2
  17.2 0.7 slice.56
  18.0 3.4 collective-permute-start
  21.4 1.3 copy.17
  22.7 0.7 pad_add_fusion
  23.4 1.4 fusion.21
  24.8 2.6 fusion.1
  27.5 2.1 fusion
  29.7 3.1 fusion.22
  32.9 2.6 convolution_convert_fusion.2
  36.1 0.5 all-gather.6.cloned.1.call-update
  36.7 0.5 all-gather.8.cloned.1.call-update
  37.7 48.6 %all-reduce.3.cloned.1.call-done = bf16[512,2048]{1,0:T(8,128)(2,1)} async-done(((bf16[512,2048]{1,0:T(8,128)(2,1)}), bf16[512,2048]{1,0:T(8,128)(2,1)}) %all-reduce.3.cloned.1.call-update) | async-done | bytes 2097168 | tf_op jit(solution)/shard_map/psum | solution.py:92
  86.3 3.1 fusion.4
  89.8 1.0 multiply_reduce_fusion
  90.9 2.4 multiply_convert_fusion
  93.2 36.4 %all-gather.4.cloned.1.call-done = bf16[2048,1408]{1,0:T(8,128)(2,1)} async-done(((bf16[256,1408]{1,0:T(8,128)(2,1)}), bf16[2048,1408]{1,0:T(8,128)(2,1)}) %all-gather.4.cloned.1.call-update) | async-done | bytes 5767184 | tf_op jit(solution)/shard_map/all_gather | solution.py:102
  129.6 6.7 %convolution_convert_fusion.1 = bf16[512,1408]{1,0:T(8,128)(2,1)S(1)} fusion(bf16[512,2048]{1,0:T(8,128)(2,1)} %multiply_convert_fusion, bf16[2048,1408]{1,0:T(8,128)(2,1)} %all-gather.4.cloned.1.call-done), kind=kOutput, calls=%fused_computation.13 | convolution fusion | flops 2953510912 | bytes 9306112 | tf_op jit(solution)/shard_map/dot_general | solution.py:100
  136.3 1.1 copy-done.10
  137.5 2.5 collective-permute-start.3
  139.9 82.1 %all-gather.6.cloned.1.call-done = bf16[2048,1408]{1,0:T(8,128)(2,1)} async-done(((bf16[256,1408]{1,0:T(8,128)(2,1)}), bf16[2048,1408]{1,0:T(8,128)(2,1)}) %all-gather.6.cloned.1.call-update) | async-done | bytes 5767184 | tf_op jit(solution)/shard_map/all_gather | solution.py:107
  222.0 6.7 %convolution_convert_fusion = bf16[512,1408]{1,0:T(8,128)(2,1)S(1)} fusion(bf16[512,2048]{1,0:T(8,128)(2,1)} %multiply_convert_fusion, bf16[2048,1408]{1,0:T(8,128)(2,1)} %all-gather.6.cloned.1.call-done), kind=kOutput, calls=%fused_computation.12 | convolution fusion | flops 2953510912 | bytes 9306112 | tf_op jit(solution)/shard_map/dot_general | solution.py:105
  228.7 2.5 collective-permute-start.4
  231.3 83.8 %all-gather.8.cloned.1.call-done = bf16[1408,2048]{1,0:T(8,128)(2,1)} async-done(((bf16[1408,256]{1,0:T(8,128)(2,1)}), bf16[1408,2048]{1,0:T(8,128)(2,1)}) %all-gather.8.cloned.1.call-update) | async-done | bytes 5767184 | tf_op jit(solution)/shard_map/all_gather | solution.py:122
  315.1 12.0 %convolution_convert_fusion.3 = bf16[512,2048]{1,0:T(8,128)(2,1)} fusion(bf16[1408,2048]{1,0:T(8,128)(2,1)} %all-gather.8.cloned.1.call-done, bf16[512,1408]{1,0:T(8,128)(2,1)} %copy-done.11, bf16[512,1408]{1,0:T(8,128)(2,1)} %copy-done.10, bf16[2,1408]{1,0:T(2,128)(2,1)S(1)} %collective-permute-done.4, bf16[2,1408]{1,0:T(2,128)(2,1)S(1)} %collective-permute-done.3, ...), kind=kOutput, calls=%fused_computation.15 | convolution fusion | flops 2984116224 | bytes 10793984 | tf_op jit(solution)/shard_map/dot_general | solution.py:120
  327.1 29.5 %reduce-scatter.2.cloned.1.call-done = bf16[512,512]{1,0:T(8,128)(2,1)} async-done(((bf16[512,2048]{1,0:T(8,128)(2,1)}), bf16[512,512]{1,0:T(8,128)(2,1)}) %reduce-scatter.2.cloned.1.call-update) | async-done | bytes 524304 | tf_op jit(solution)/shard_map/reduce_scatter | solution.py:125
  356.6 1.5 fusion.25
  358.2 5.8 %all-reduce = (f32[512]{0:T(512)S(1)}, f32[512]{0:T(512)S(1)}) all-reduce(f32[512]{0:T(512)S(1)} %get-tuple-element.6, f32[512]{0:T(512)S(1)} %get-tuple-element.5), channel_id=1, replica_groups=mesh['sp'=8,'tp'=4] {'tp'}, use_global_device_ids=true, to_apply=%region_9.10 | all-reduce | flops 1024 | bytes 8192 | tf_op jit(solution)/shard_map/psum | solution.py:129
  363.9 2.3 multiply_convert_fusion.1
  (50 shorter events, 1.8 us)
Async XLA Ops:
  7.4 25.5 %copy-start = (bf16[512,2048]{1,0:T(8,128)(2,1)S(1)}, bf16[512,2048]{1,0:T(8,128)(2,1)}, u32[]{:S(2)}) copy-start(bf16[512,2048]{1,0:T(8,128)(2,1)} %param.20) | copy-start | bytes 6291460
  7.4 78.9 %all-reduce.3.cloned.1.call-start = ((), (), s32[]{:S(2)}) async-start(), calls=%async_computation.1 | async-start | bytes 4194304 | tf_op jit(solution)/shard_map/psum | solution.py:92
  8.2 14.5 %collective-permute-start.1 = (s32[128]{0:T(128)S(1)}, s32[128]{0:T(128)S(1)}, u32[]{:S(2)}, u32[]{:S(2)}) collective-permute-start(s32[128]{0:T(128)S(1)} %slice.57), channel_id=1, source_target_pairs={{0,4},{4,8},{8,12},{12,16},{16,20},{20,24},{24,28},{1,5},{5,9},{9,... | collective-permute-start | bytes 1544 | tf_op jit(solution)/shard_map/ppermute | solution.py:17
  13.8 11.0 %collective-permute-start.2 = (bf16[128,64]{0,1:T(8,128)(2,1)S(1)}, bf16[128,64]{0,1:T(8,128)(2,1)S(1)}, u32[]{:S(2)}, u32[]{:S(2)}) collective-permute-start(bf16[128,64]{0,1:T(8,128)(2,1)S(1)} %slice.58), channel_id=1, source_target_pairs={{0,4},{4,8},{8,12},{12,16},{16,20},{20,24},{24,28},{1,5},{5,9},{9,... | collective-permute-start | bytes 49160 | tf_op jit(solution)/shard_map/ppermute | solution.py:17
  18.0 11.7 %collective-permute-start = (bf16[128,64]{0,1:T(8,128)(2,1)S(1)}, bf16[128,64]{0,1:T(8,128)(2,1)S(1)}, u32[]{:S(2)}, u32[]{:S(2)}) collective-permute-start(bf16[128,64]{0,1:T(8,128)(2,1)S(1)} %slice.56), channel_id=1, source_target_pairs={{0,4},{4,8},{8,12},{12,16},{16,20},{20,24},{24,28},{1,5},{5,9},{9,... | collective-permute-start | bytes 49160 | tf_op jit(solution)/shard_map/ppermute | solution.py:17
  24.8 2.6 copy-start.9
  27.5 2.2 copy-start.7
  35.5 2.0 copy-start.4
  35.5 2.0 copy-start.5
  35.5 2.2 copy-start.3
  35.5 94.1 %all-gather.4.cloned.1.call-start = ((), (), s32[]{:S(2)}) async-start(), calls=%async_computation.2 | async-start | bytes 6488064 | tf_op jit(solution)/shard_map/all_gather | solution.py:102
  36.1 185.9 %all-gather.6.cloned.1.call-start = ((), (), s32[]{:S(2)}) async-start(), calls=%async_computation.3 | async-start | bytes 6488064 | tf_op jit(solution)/shard_map/all_gather | solution.py:107
  36.7 278.4 %all-gather.8.cloned.1.call-start = ((), (), s32[]{:S(2)}) async-start(), calls=%async_computation.4 | async-start | bytes 6488064 | tf_op jit(solution)/shard_map/all_gather | solution.py:122
  37.2 319.4 %reduce-scatter.2.cloned.1.call-start = ((), (), s32[]{:S(2)}) async-start(), calls=%async_computation.5 | async-start | bytes 2621440 | tf_op jit(solution)/shard_map/reduce_scatter | solution.py:125
  86.3 3.1 copy-start.1
  86.3 3.5 copy-start.2
  89.4 1.4 copy-start.6
  136.3 1.1 copy-start.10
  137.5 177.6 %collective-permute-start.3 = (bf16[2,1408]{1,0:T(2,128)(2,1)S(1)}, bf16[2,1408]{1,0:T(2,128)(2,1)S(1)}, u32[]{:S(2)}, u32[]{:S(2)}) collective-permute-start(bf16[2,1408]{1,0:T(2,128)(2,1)S(1)} %slice.74), channel_id=1, source_target_pairs={{0,4},{4,8},{8,12},{12,16},{16,20},{20,24},{24,28},{1,5},{5,9},{9,... | collective-permute-start | bytes 16904 | tf_op jit(solution)/shard_map/ppermute | solution.py:17
  228.7 2.5 copy-start.11
  228.7 86.3 %collective-permute-start.4 = (bf16[2,1408]{1,0:T(2,128)(2,1)S(1)}, bf16[2,1408]{1,0:T(2,128)(2,1)S(1)}, u32[]{:S(2)}, u32[]{:S(2)}) collective-permute-start(bf16[2,1408]{1,0:T(2,128)(2,1)S(1)} %slice.77), channel_id=1, source_target_pairs={{0,4},{4,8},{8,12},{12,16},{16,20},{20,24},{24,28},{1,5},{5,9},{9,... | collective-permute-start | bytes 16904 | tf_op jit(solution)/shard_map/ppermute | solution.py:17
  327.1 36.8 %copy-start.8 = (f32[512]{0:T(512)S(1)}, f32[512]{0:T(512)}, u32[]{:S(2)}) copy-start(f32[512]{0:T(512)} %param.27) | copy-start | bytes 6148
Sparse Core Ops, SparseCore 0:
  35.6 50.6 all-reduce.2
  327.2 29.3 reduce-scatter.1
Sparse Core Ops, SparseCore 1:
  38.2 91.4 all-gather.3
  131.7 90.3 all-gather.5
  223.9 91.1 all-gather.7
where the time goes:
time: 374 us
  waiting for transfers between devices  282 us (75%)
  matrix products  33.7 us (9%)
  starting transfers between devices  17 us (5%)
  between operations  15.3 us (4%)
  other arithmetic  14.9 us (4%)
  blocking collectives  5.76 us (2%)
  local copies, waits for them, and re-layouts  5.23 us (1%)
    all_gather x1, waiting for transfers between devices, on_device(): lax.all_gather(down_proj, 'sp', axis=1, tiled=True)  83.8 us
    all_gather x1, waiting for transfers between devices, on_device(): lax.all_gather(value_proj, 'sp', axis=0, tiled=True)  82.1 us
    psum x1, waiting for transfers between devices, on_device(): lax.psum(partial_value.astype(jnp.bfloat16), 'tp').astype(jnp.float32)  48.6 us
    all_gather x1, waiting for transfers between devices, on_device(): lax.all_gather(gate_proj, 'sp', axis=0, tiled=True)  36.4 us
    reduce_scatter x1, waiting for transfers between devices, on_device(): lax.psum_scatter(terms.astype(jnp.bfloat16), 'tp', scatter_dimension=1, t...  29.5 us
    ppermute x5, starting transfers between devices, passed_along(): return lax.ppermute(block, axis, route)  16.6 us
    dot_general x1, matrix products, on_device(): jnp.dot(hidden, lax.all_gather(down_proj, 'sp', axis=1, tiled=True), pref...  12 us
  transfers between devices with their start and end apart: 10, of which 5 were waited for; matrix products, arithmetic and copies ran while one was open for 8% of the time, Pallas kernels for 0%

commit v1 on v0

--- a/solution.py
+++ b/solution.py
@@ -3,12 +3,18 @@
 import jax.numpy as jnp
 from jax import lax
 from jax.sharding import PartitionSpec as P
+from jax.lax import all_gather
 
 HD = 64
 WIN = 128
 TAPS = 3
 mix_scale = math.sqrt(2.0)
 norm_eps = 1e-05
+
+
+def end_keys(mine):
+    part_next = jnp.sum(all_gather(mine, "tp"), axis=0)
+    return part_next
 
 
 def passed_along(block, axis, distance):
@@ -89,7 +95,7 @@
     width = residual.shape[1]
     share = width // lax.axis_size("tp")
     col_start = lax.axis_index("tp") * share
-    attn_total = lax.psum(partial_value.astype(jnp.bfloat16), "tp").astype(jnp.float32)
+    attn_total = end_keys(partial_value.astype(jnp.bfloat16)).astype(jnp.float32)
     first_sum = mix_scale * residual.astype(jnp.float32) + attn_total
     mean = jnp.mean(first_sum, axis=1, keepdims=True)
     var = jnp.mean(jnp.square(first_sum - mean), axis=1, keepdims=True)

time: 374 us -> 431 us (1.15)
  waiting for transfers between devices: 282 us -> 333 us
  other arithmetic: 14.9 us -> 22.3 us
    all_gather x0 -> x1, waiting for transfers between devices: none -> 55.1 us  [end_keys(): part_next = jnp.sum(all_gather(mine, 'tp'), axis=0)]
    psum x1 -> x0, waiting for transfers between devices: 48.6 us -> none  [on_device(): lax.psum(partial_value.astype(jnp.bfloat16), 'tp').astype(jnp.float32)]
    all_gather x1, waiting for transfers between devices: 36.4 us -> 79.9 us  [on_device(): lax.all_gather(gate_proj, 'sp', axis=0, tiled=True)]
    reduce_sum x0 -> x1, other arithmetic: none -> 7.25 us  [end_keys(): part_next = jnp.sum(all_gather(mine, 'tp'), axis=0)]
  transfers between devices with their start and end apart: 10 -> 10, of which waited for: 5 -> 5; matrix products, arithmetic and copies ran while one was open for 8% -> 9% of each run, Pallas kernels for 0% -> 0%
where the time goes in v1:
time: 431 us
  waiting for transfers between devices  333 us (77%)
  matrix products  33.8 us (8%)
  other arithmetic  22.3 us (5%)
  starting transfers between devices  17.2 us (4%)
  between operations  13.4 us (3%)
  blocking collectives  5.76 us (1%)
  local copies, waits for them, and re-layouts  5.53 us (1%)
    all_gather x1, waiting for transfers between devices, on_device(): lax.all_gather(down_proj, 'sp', axis=1, tiled=True)  83.8 us
    all_gather x1, waiting for transfers between devices, on_device(): lax.all_gather(value_proj, 'sp', axis=0, tiled=True)  82.5 us
    all_gather x1, waiting for transfers between devices, on_device(): lax.all_gather(gate_proj, 'sp', axis=0, tiled=True)  79.9 us
    all_gather x1, waiting for transfers between devices, end_keys(): part_next = jnp.sum(all_gather(mine, 'tp'), axis=0)  55.1 us
    reduce_scatter x1, waiting for transfers between devices, on_device(): lax.psum_scatter(terms.astype(jnp.bfloat16), 'tp', scatter_dimension=1, t...  29.5 us
    ppermute x5, starting transfers between devices, passed_along(): return lax.ppermute(block, axis, route)  16.9 us
    dot_general x1, matrix products, on_device(): jnp.dot(hidden, lax.all_gather(down_proj, 'sp', axis=1, tiled=True), pref...  12.1 us
  transfers between devices with their start and end apart: 10, of which 5 were waited for; matrix products, arithmetic and copies ran while one was open for 9% of the time, Pallas kernels for 0%

profile of v1, /device:TPU:0, one launch (start us, length us, event | category | flops | bytes accessed | tf_op | source)
XLA Modules:
  0.0 430.8 jit_solution(1563224913976553067)
XLA Ops:
  6.5 0.8 slice.57
  7.4 4.9 %collective-permute-start.1 = (s32[128]{0:T(128)S(1)}, s32[128]{0:T(128)S(1)}, u32[]{:S(2)}, u32[]{:S(2)}) collective-permute-start(s32[128]{0:T(128)S(1)} %slice.57), channel_id=1, source_target_pairs={{0,4},{4,8},{8,12},{12,16},{16,20},{20,24},{24,28},{1,5},{5,9},{9,... | collective-permute-start | bytes 1544 | tf_op jit(solution)/shard_map/ppermute | solution.py:23
  12.3 0.7 slice.58
  13.0 3.4 collective-permute-start.2
  16.4 0.7 slice.56
  17.1 3.4 collective-permute-start
  20.6 1.3 copy.17
  21.9 0.7 pad_add_fusion
  22.6 1.4 fusion.21
  24.0 2.6 fusion.1
  26.7 2.1 fusion
  28.9 3.1 fusion.22
  32.0 2.7 convolution_convert_fusion.2
  34.8 0.7 all-gather.6.cloned.1.call-update
  37.3 55.1 %all-gather.12.cloned.1.call-done = bf16[2048,2048]{1,0:T(8,128)(2,1)} async-done(((bf16[512,2048]{1,0:T(8,128)(2,1)}), bf16[2048,2048]{1,0:T(8,128)(2,1)}) %all-gather.12.cloned.1.call-update) | async-done | bytes 8388624 | tf_op jit(solution)/shard_map/all_gather | solution.py:16
  92.4 7.3 %reduce_sum.58 = bf16[512,2048]{1,0:T(8,128)(2,1)} reduce(bf16[4,512,2048]{2,1,0:T(8,128)(2,1)} %bitcast.43, bf16[]{:T(256)} %constant.15.clone.1), dimensions={0}, to_apply=%region_2.3 | reduce | flops 3145728 | bytes 10485762 | tf_op jit(solution)/shard_map/reduce_sum | solution.py:16
  99.7 3.3 fusion.4
  103.7 1.0 multiply_reduce_fusion
  104.7 2.4 multiply_convert_fusion
  107.1 79.9 %all-gather.6.cloned.1.call-done = bf16[2048,1408]{1,0:T(8,128)(2,1)} async-done(((bf16[256,1408]{1,0:T(8,128)(2,1)}), bf16[2048,1408]{1,0:T(8,128)(2,1)}) %all-gather.6.cloned.1.call-update) | async-done | bytes 5767184 | tf_op jit(solution)/shard_map/all_gather | solution.py:108
  187.0 6.7 %convolution_convert_fusion.1 = bf16[512,1408]{1,0:T(8,128)(2,1)S(1)} fusion(bf16[512,2048]{1,0:T(8,128)(2,1)} %multiply_convert_fusion, bf16[2048,1408]{1,0:T(8,128)(2,1)} %all-gather.6.cloned.1.call-done), kind=kOutput, calls=%fused_computation.13 | convolution fusion | flops 2953510912 | bytes 9306112 | tf_op jit(solution)/shard_map/dot_general | solution.py:106
  193.7 1.1 copy-done.10
  194.8 2.5 collective-permute-start.3
  197.2 82.5 %all-gather.8.cloned.1.call-done = bf16[2048,1408]{1,0:T(8,128)(2,1)} async-done(((bf16[256,1408]{1,0:T(8,128)(2,1)}), bf16[2048,1408]{1,0:T(8,128)(2,1)}) %all-gather.8.cloned.1.call-update) | async-done | bytes 5767184 | tf_op jit(solution)/shard_map/all_gather | solution.py:113
  279.7 6.7 %convolution_convert_fusion = bf16[512,1408]{1,0:T(8,128)(2,1)S(1)} fusion(bf16[512,2048]{1,0:T(8,128)(2,1)} %multiply_convert_fusion, bf16[2048,1408]{1,0:T(8,128)(2,1)} %all-gather.8.cloned.1.call-done), kind=kOutput, calls=%fused_computation.12 | convolution fusion | flops 2953510912 | bytes 9306112 | tf_op jit(solution)/shard_map/dot_general | solution.py:111
  286.4 2.7 collective-permute-start.4
  289.2 83.8 %all-gather.10.cloned.1.call-done = bf16[1408,2048]{1,0:T(8,128)(2,1)} async-done(((bf16[1408,256]{1,0:T(8,128)(2,1)}), bf16[1408,2048]{1,0:T(8,128)(2,1)}) %all-gather.10.cloned.1.call-update) | async-done | bytes 5767184 | tf_op jit(solution)/shard_map/all_gather | solution.py:128
  373.1 12.1 %convolution_convert_fusion.3 = bf16[512,2048]{1,0:T(8,128)(2,1)} fusion(bf16[1408,2048]{1,0:T(8,128)(2,1)} %all-gather.10.cloned.1.call-done, bf16[512,1408]{1,0:T(8,128)(2,1)} %copy-done.11, bf16[512,1408]{1,0:T(8,128)(2,1)} %copy-done.10, bf16[2,1408]{1,0:T(2,128)(2,1)S(1)} %collective-permute-done.4, bf16[2,1408]{1,0:T(2,128)(2,1)S(1)} %collective-permute-done.3, ...), kind=kOutput, calls=%fused_computation.15 | convolution fusion | flops 2984116224 | bytes 10793984 | tf_op jit(solution)/shard_map/dot_general | solution.py:126
  385.2 29.5 %reduce-scatter.2.cloned.1.call-done = bf16[512,512]{1,0:T(8,128)(2,1)} async-done(((bf16[512,2048]{1,0:T(8,128)(2,1)}), bf16[512,512]{1,0:T(8,128)(2,1)}) %reduce-scatter.2.cloned.1.call-update) | async-done | bytes 524304 | tf_op jit(solution)/shard_map/reduce_scatter | solution.py:131
  414.7 1.5 fusion.25
  416.2 5.8 %all-reduce = (f32[512]{0:T(512)S(1)}, f32[512]{0:T(512)S(1)}) all-reduce(f32[512]{0:T(512)S(1)} %get-tuple-element.6, f32[512]{0:T(512)S(1)} %get-tuple-element.5), channel_id=1, replica_groups=mesh['sp'=8,'tp'=4] {'tp'}, use_global_device_ids=true, to_apply=%region_9.10 | all-reduce | flops 1024 | bytes 8192 | tf_op jit(solution)/shard_map/psum | solution.py:135
  422.0 2.3 multiply_convert_fusion.1
  (51 shorter events, 2.8 us)
Async XLA Ops:
  6.5 25.5 %copy-start = (bf16[512,2048]{1,0:T(8,128)(2,1)S(1)}, bf16[512,2048]{1,0:T(8,128)(2,1)}, u32[]{:S(2)}) copy-start(bf16[512,2048]{1,0:T(8,128)(2,1)} %param.20) | copy-start | bytes 6291460
  6.5 85.9 %all-gather.12.cloned.1.call-start = ((), (), s32[]{:S(2)}) async-start(), calls=%async_computation.5 | async-start | bytes 10485760 | tf_op jit(solution)/shard_map/all_gather | solution.py:16
  7.4 14.5 %collective-permute-start.1 = (s32[128]{0:T(128)S(1)}, s32[128]{0:T(128)S(1)}, u32[]{:S(2)}, u32[]{:S(2)}) collective-permute-start(s32[128]{0:T(128)S(1)} %slice.57), channel_id=1, source_target_pairs={{0,4},{4,8},{8,12},{12,16},{16,20},{20,24},{24,28},{1,5},{5,9},{9,... | collective-permute-start | bytes 1544 | tf_op jit(solution)/shard_map/ppermute | solution.py:23
  13.0 11.0 %collective-permute-start.2 = (bf16[128,64]{0,1:T(8,128)(2,1)S(1)}, bf16[128,64]{0,1:T(8,128)(2,1)S(1)}, u32[]{:S(2)}, u32[]{:S(2)}) collective-permute-start(bf16[128,64]{0,1:T(8,128)(2,1)S(1)} %slice.58), channel_id=1, source_target_pairs={{0,4},{4,8},{8,12},{12,16},{16,20},{20,24},{24,28},{1,5},{5,9},{9,... | collective-permute-start | bytes 49160 | tf_op jit(solution)/shard_map/ppermute | solution.py:23
  17.1 11.7 %collective-permute-start = (bf16[128,64]{0,1:T(8,128)(2,1)S(1)}, bf16[128,64]{0,1:T(8,128)(2,1)S(1)}, u32[]{:S(2)}, u32[]{:S(2)}) collective-permute-start(bf16[128,64]{0,1:T(8,128)(2,1)S(1)} %slice.56), channel_id=1, source_target_pairs={{0,4},{4,8},{8,12},{12,16},{16,20},{20,24},{24,28},{1,5},{5,9},{9,... | collective-permute-start | bytes 49160 | tf_op jit(solution)/shard_map/ppermute | solution.py:23
  24.0 2.6 copy-start.9
  26.7 2.2 copy-start.7
  34.7 2.3 copy-start.4
  34.7 2.3 copy-start.5
  34.7 2.5 copy-start.3
  34.7 152.2 %all-gather.6.cloned.1.call-start = ((), (), s32[]{:S(2)}) async-start(), calls=%async_computation.1 | async-start | bytes 6488064 | tf_op jit(solution)/shard_map/all_gather | solution.py:108
  35.5 244.2 %all-gather.8.cloned.1.call-start = ((), (), s32[]{:S(2)}) async-start(), calls=%async_computation.2 | async-start | bytes 6488064 | tf_op jit(solution)/shard_map/all_gather | solution.py:113
  36.2 336.8 %all-gather.10.cloned.1.call-start = ((), (), s32[]{:S(2)}) async-start(), calls=%async_computation.3 | async-start | bytes 6488064 | tf_op jit(solution)/shard_map/all_gather | solution.py:128
  36.8 377.9 %reduce-scatter.2.cloned.1.call-start = ((), (), s32[]{:S(2)}) async-start(), calls=%async_computation.4 | async-start | bytes 2621440 | tf_op jit(solution)/shard_map/reduce_scatter | solution.py:131
  99.7 3.3 copy-start.1
  99.7 4.0 copy-start.2
  102.9 1.7 copy-start.6
  193.7 1.1 copy-start.10
  194.8 178.3 %collective-permute-start.3 = (bf16[2,1408]{1,0:T(2,128)(2,1)S(1)}, bf16[2,1408]{1,0:T(2,128)(2,1)S(1)}, u32[]{:S(2)}, u32[]{:S(2)}) collective-permute-start(bf16[2,1408]{1,0:T(2,128)(2,1)S(1)} %slice.74), channel_id=1, source_target_pairs={{0,4},{4,8},{8,12},{12,16},{16,20},{20,24},{24,28},{1,5},{5,9},{9,... | collective-permute-start | bytes 16904 | tf_op jit(solution)/shard_map/ppermute | solution.py:23
  286.4 2.7 copy-start.11
  286.4 86.6 %collective-permute-start.4 = (bf16[2,1408]{1,0:T(2,128)(2,1)S(1)}, bf16[2,1408]{1,0:T(2,128)(2,1)S(1)}, u32[]{:S(2)}, u32[]{:S(2)}) collective-permute-start(bf16[2,1408]{1,0:T(2,128)(2,1)S(1)} %slice.77), channel_id=1, source_target_pairs={{0,4},{4,8},{8,12},{12,16},{16,20},{20,24},{24,28},{1,5},{5,9},{9,... | collective-permute-start | bytes 16904 | tf_op jit(solution)/shard_map/ppermute | solution.py:23
  385.2 36.8 %copy-start.8 = (f32[512]{0:T(512)S(1)}, f32[512]{0:T(512)}, u32[]{:S(2)}) copy-start(f32[512]{0:T(512)} %param.27) | copy-start | bytes 6148
Sparse Core Ops, SparseCore 0:
  34.9 57.5 all-gather.11
  94.6 92.3 all-gather.5
  189.2 90.5 all-gather.7
  281.6 91.3 all-gather.9
  385.3 29.3 reduce-scatter.1
